TPU v7x, 32 devices: a whole 2x2x4 slice. The times are simulated.
32 devices in a mesh: sp: 8 (over z, x), tp: 4 (over y, core).
Axes of the slice: x: 2, y: 2, z: 4, core: 2. Of those that a mesh axis runs over, the one named last changes fastest.
Arguments:
- tokens: bfloat16 [8, 80, 4096], P(None, 'sp', 'tp'), may hold values from -6 to 6
- latent_down_weight: bfloat16 [4096, 512], replicated, may hold values from -0.09375 to 0.09375
- w_rope_key: bfloat16 [4096, 64], replicated, may hold values from -0.09375 to 0.09375
- latent_norm_gain: float32 [512], replicated, may hold values from 0.1 to 1.9
- key_up_weight: bfloat16 [512, 4096], P(None, 'tp'), may hold values from -0.25 to 0.25
- value_up_weight: bfloat16 [512, 4096], P(None, 'tp'), may hold values from -0.25 to 0.25
- cached_latent_rows: bfloat16 [8, 32768, 512], P('sp', 'tp'), may hold values from -6 to 6
- past_rope: bfloat16 [8, 32768, 64], P('sp', 'tp'), may hold values from -6 to 6
- query_nope: bfloat16 [8, 4096], P('sp', 'tp'), may hold values from -8 to 8
- query_rope: bfloat16 [8, 2048], P('sp', 'tp'), may hold values from -300 to 300
Outputs:
- new_keys: bfloat16 [8, 80, 4096], P('sp', None, 'tp')
- new_values: bfloat16 [8, 80, 4096], P('sp', None, 'tp')
- new_rope: bfloat16 [8, 80, 64], P('sp')
- attended: bfloat16 [8, 4096], P('sp', 'tp')
All inputs are finite; a program needn't handle non-finite values.
Results may differ from a plain program's by a relative error of at most 0.0085.
Values may be sent and summed in bfloat16 or wider, within the bound.
A program may use at most 64 MiB of HBM per device.

v0:
```python
import jax
import jax.numpy as jnp
from jax import lax
from jax.sharding import PartitionSpec as P

PLAIN_KEY_WIDTH = 128
ROPE = 64
VALUE_WIDTH = 128
PAST_POSITIONS = 32768
epsilon = 1e-06
rope_theta = 10000.0


def combined_all(part, axis, combine):
    gathered = jax.tree.map(lambda a: lax.all_gather(a, axis), part)

    def take(source):
        return jax.tree.map(lambda a: lax.dynamic_index_in_dim(a, source, 0, False), gathered)

    return lax.fori_loop(
        1, lax.axis_size(axis), lambda source, state: combine(state, take(source)), take(0)
    )


def rotate(values, positions):
    halfway = values.shape[-1] // 2
    frequency = rope_theta ** (-jnp.arange(halfway, dtype=jnp.float32) / halfway)
    angles = positions[:, None] * frequency
    first = values[..., :halfway]
    second = values[..., halfway:]
    return jnp.concatenate(
        [
            first * jnp.cos(angles) - second * jnp.sin(angles),
            first * jnp.sin(angles) + second * jnp.cos(angles),
        ],
        axis=-1,
    )


def combine_parts(first, second):
    highest = jnp.maximum(first[0], second[0])
    scale_first = jnp.exp(first[0] - highest)
    scale_second = jnp.exp(second[0] - highest)
    total = first[1] * scale_first + second[1] * scale_second
    summed = first[2] * scale_first[..., None] + second[2] * scale_second[..., None]
    return (highest, total, summed)


def on_device(
    tokens,
    latent_down_weight,
    w_rope_key,
    latent_norm_gain,
    key_up_weight,
    value_up_weight,
    cached_latent_rows,
    past_rope,
    query_nope,
    query_rope,
):
    rows_here = lax.all_to_all(tokens, "sp", split_axis=0, concat_axis=1, tiled=True)
    prompts, per_seq, features = rows_here.shape
    row_count = prompts * per_seq
    latent_width = latent_down_weight.shape[1]
    turn_width = w_rope_key.shape[1]
    factor = (PLAIN_KEY_WIDTH + ROPE) ** (-0.5)
    fragment = lax.all_gather(rows_here, "tp", axis=2, tiled=True)
    columns = fragment.shape[2]
    flat_rows = fragment.reshape(row_count, columns)
    latent_raw = jnp.dot(flat_rows, latent_down_weight, preferred_element_type=jnp.float32)
    rope_raw = jnp.dot(flat_rows, w_rope_key, preferred_element_type=jnp.float32)
    scale = lax.rsqrt(jnp.mean(latent_raw * latent_raw, axis=-1, keepdims=True) + epsilon)
    latent = (latent_raw * scale * latent_norm_gain).astype(jnp.bfloat16)
    positions = (PAST_POSITIONS + jnp.arange(per_seq)).astype(jnp.float32)
    rope_local = rotate(rope_raw.reshape(prompts, per_seq, turn_width), positions).astype(
        jnp.bfloat16
    )
    keys_local = (
        jnp.dot(latent, key_up_weight, preferred_element_type=jnp.float32)
        .astype(jnp.bfloat16)
        .reshape(prompts, per_seq, key_up_weight.shape[1])
    )
    values_local = (
        jnp.dot(latent, value_up_weight, preferred_element_type=jnp.float32)
        .astype(jnp.bfloat16)
        .reshape(prompts, per_seq, value_up_weight.shape[1])
    )
    new_keys, new_values, new_rope = (keys_local, values_local, rope_local)
    owned = query_nope.shape[0]
    heads_local = query_nope.shape[1] // PLAIN_KEY_WIDTH
    query_own = query_nope.reshape(owned, heads_local, PLAIN_KEY_WIDTH)
    turn_own = query_rope.reshape(owned, heads_local, ROPE)
    head_keys = key_up_weight.reshape(latent_width, heads_local, PLAIN_KEY_WIDTH)
    query_latent = jnp.einsum(
        "shd,khd->shk", query_own, head_keys, preferred_element_type=jnp.float32
    ).astype(jnp.bfloat16)
    every_latent, every_turn = (
        lax.all_gather(query_latent, "tp", axis=1, tiled=True),
        lax.all_gather(turn_own, "tp", axis=1, tiled=True),
    )
    past_scores = jnp.einsum(
        "shk,spk->shp", every_latent, cached_latent_rows, preferred_element_type=jnp.float32
    )
    past_scores = (
        past_scores
        + jnp.einsum("shd,spd->shp", every_turn, past_rope, preferred_element_type=jnp.float32)
    ) * factor
    local_peak = jnp.max(past_scores, axis=-1)
    local_weight = jnp.exp(past_scores - local_peak[:, :, None])
    local_total = jnp.sum(local_weight, axis=-1)
    local_latent = jnp.einsum(
        "shp,spk->shk",
        local_weight.astype(jnp.bfloat16),
        cached_latent_rows,
        preferred_element_type=jnp.float32,
    )
    peak_all, total_all, latent_all = combined_all(
        (local_peak, local_total, local_latent), "tp", combine_parts
    )
    start = lax.axis_index("tp") * heads_local
    past_peak = lax.dynamic_slice_in_dim(peak_all, start, heads_local, 1)
    past_total = lax.dynamic_slice_in_dim(total_all, start, heads_local, 1)
    past_sum = lax.dynamic_slice_in_dim(latent_all, start, heads_local, 1)
    fresh = new_keys.shape[1]
    new_scores = jnp.einsum(
        "shd,sphd->shp",
        query_own,
        new_keys.reshape(owned, fresh, heads_local, PLAIN_KEY_WIDTH),
        preferred_element_type=jnp.float32,
    )
    new_scores = (
        new_scores
        + jnp.einsum("shd,spd->shp", turn_own, new_rope, preferred_element_type=jnp.float32)
    ) * factor
    peak = jnp.maximum(past_peak, jnp.max(new_scores, axis=-1))
    past_share = jnp.exp(past_peak - peak)
    new_weight = jnp.exp(new_scores - peak[:, :, None])
    denominator = past_total * past_share + jnp.sum(new_weight, axis=-1)
    latent_sum = (past_sum * past_share[..., None]).astype(jnp.bfloat16)
    head_values = value_up_weight.reshape(latent_width, heads_local, VALUE_WIDTH)
    past_out = jnp.einsum(
        "shk,khd->shd", latent_sum, head_values, preferred_element_type=jnp.float32
    )
    new_out = jnp.einsum(
        "shp,sphd->shd",
        new_weight.astype(jnp.bfloat16),
        new_values.reshape(owned, fresh, heads_local, VALUE_WIDTH),
        preferred_element_type=jnp.float32,
    )
    attended = (
        ((past_out + new_out) / denominator[:, :, None])
        .astype(jnp.bfloat16)
        .reshape(owned, heads_local * VALUE_WIDTH)
    )
    return (new_keys, new_values, new_rope, attended)


def solution(mesh):
    in_specs = (
        P(None, "sp", "tp"),
        P(),
        P(),
        P(),
        P(None, "tp"),
        P(None, "tp"),
        P("sp", "tp", None),
        P("sp", "tp", None),
        P("sp", "tp"),
        P("sp", "tp"),
    )
    out_specs = (P("sp", None, "tp"), P("sp", None, "tp"), P("sp", None, None), P("sp", "tp"))
    return jax.shard_map(
        on_device, mesh=mesh, in_specs=in_specs, out_specs=out_specs, check_vma=False
    )
```

profile of v0, /device:TPU:0, one launch (start us, length us, event | category | flops | bytes accessed | tf_op | source)
XLA Modules:
  0.0 66.8 jit_solution(9695988542635753334)
XLA Ops:
  0.6 0.0 copy-start
  0.6 1.8 %copy.21 = bf16[8,10,1024]{2,1,0:T(8,128)(2,1)} copy(bf16[8,10,1024]{2,0,1:T(8,128)(2,1)} %param.12) | data formatting | bytes 327680 | tf_op args[0]
  2.4 7.3 %all-to-all-start = ((bf16[8,10,1024]{2,1,0:T(8,128)(2,1)}), bf16[8,10,1024]{2,1,0:T(8,128)(2,1)}, u32[]{:S(2)}, u32[]{:S(2)}) async-start(bf16[8,10,1024]{2,1,0:T(8,128)(2,1)} %copy.21), calls=%async_computation | async-start | bytes 524288 | tf_op jit(solution)/shard_map/all_to_all | solution.py:61
  9.7 0.7 %reduce.8 = bf16[512]{0:T(512)(128)(2,1)S(1)} reduce(bf16[1,512]{1,0:T(2,128)(2,1)} %param.21, bf16[]{:T(256)} %constant.97), dimensions={0}, to_apply=%param.21.reduce_sub_computation | reduce | bytes 2050 | tf_op args[9]
  10.4 0.1 reshape.326
  10.5 5.2 %all_gather.29 = bf16[1,32,64]{2,1,0:T(8,128)(2,1)S(1)} all-gather(bf16[1,8,64]{2,1,0:T(8,128)(2,1)S(1)} %reshape.326), channel_id=1, replica_groups=mesh['sp'=8,'tp'=4] {'tp'}, dimensions={1}, use_global_device_ids=true | all-gather | bytes 5120 | tf_op jit(solution)/shard_map/all_gather | solution.py:99
  15.7 1.6 %fusion.18 = bf16[8,1,512]{2,1,0:T(2,128)(2,1)S(1)} fusion(bf16[1,1024]{1,0:T(2,128)(2,1)} %param.20, bf16[512,1024]{1,0:T(8,128)(2,1)} %param.16), kind=kOutput, calls=%fused_computation.28 | convolution fusion | flops 1048576 | bytes 1058816 | tf_op jit(solution)/shard_map/shd,khd->shk/dot_general | solution.py:94
  17.3 5.2 %all-gather = bf16[32,512]{1,0:T(8,128)(2,1)S(1)} all-gather(bf16[8,512]{1,0:T(8,128)(2,1)S(1)} %bitcast.161), channel_id=2, replica_groups=mesh['sp'=8,'tp'=4] {'tp'}, dimensions={0}, use_global_device_ids=true | all-gather | bytes 40960 | tf_op jit(solution)/shard_map/all_gather | solution.py:98
  22.5 0.0 copy-start.7
  22.5 5.9 %fusion.11 = f32[32,8192]{1,0:T(8,128)S(1)} fusion(bf16[32,512]{1,0:T(8,128)(2,1)S(1)} %all-gather, bf16[1,8192,512]{2,1,0:T(8,128)(2,1)} %param.18), kind=kOutput, calls=%fused_computation.17 | convolution fusion | flops 268435456 | bytes 9469952 | tf_op jit(solution)/shard_map/shk,spk->shp/dot_general | solution.py:101
  28.4 0.0 copy-done
  28.4 0.4 fusion.64
  28.8 0.4 fusion.23
  29.2 0.0 copy-done.7
  29.2 0.6 dynamic-slice
  30.5 0.2 dynamic-update-slice
  30.7 0.2 dynamic-update-slice.1
  30.9 7.1 %all-reduce.2 = (f32[128]{0:T(128)S(1)}, f32[128]{0:T(128)S(1)}) all-reduce(f32[128]{0:T(128)S(1)} %dynamic-update-slice, f32[128]{0:T(128)S(1)} %dynamic-update-slice.1), channel_id=3, replica_groups=mesh['sp'=8,'tp'=4] {'tp'}, use_global_device_ids=true, to_apply=%add | all-reduce | flops 256 | bytes 2048
  38.0 0.1 reshape.336
  38.1 0.1 reshape.337
  38.2 0.0 copy-start.1
  38.2 0.0 copy-start.5
  38.2 5.1 %fusion.9 = f32[32,512]{1,0:T(8,128)S(1)} fusion(bf16[1,8192,512]{2,1,0:T(8,128)(2,1)} %param.18, f32[32,8192]{1,0:T(8,128)S(1)} %get-tuple-element.237, f32[32]{0:T(128)S(1)} %get-tuple-element.236), kind=kOutput, calls=%fused_computation.15 | convolution fusion | flops 268959744 | bytes 9502848 | tf_op jit(solution)/shard_map/shp,spk->shk/dot_general | solution.py:111
  43.2 0.0 copy-start.6
  43.2 0.0 copy-start.2
  43.2 5.9 %all-gather.3 = f32[128,512]{1,0:T(8,128)S(1)} all-gather(f32[32,512]{1,0:T(8,128)S(1)} %fusion.9), channel_id=5, replica_groups=mesh['sp'=8,'tp'=4] {'tp'}, dimensions={0}, use_global_device_ids=true | all-gather | bytes 327680 | tf_op jit(solution)/shard_map/all_gather | solution.py:15
  49.2 0.5 while.19
  49.2 0.1 fusion.80
  49.4 0.1 fusion.80
  49.5 0.1 fusion.80
  49.6 0.1 reshape.330
  49.7 0.0 all-to-all-done
  49.7 1.0 %all_to_all.10 = bf16[1,80,1024]{2,1,0:T(8,128)(2,1)S(1)} reshape(bf16[8,10,1024]{2,1,0:T(8,128)(2,1)} %all-to-all-done) | data formatting | bytes 327680 | tf_op jit(solution)/shard_map/all_to_all | solution.py:61
  50.7 8.0 %all_gather.27 = bf16[1,80,4096]{2,1,0:T(8,128)(2,1)S(1)} all-gather(bf16[1,80,1024]{2,1,0:T(8,128)(2,1)S(1)} %all_to_all.10), channel_id=1, replica_groups=mesh['sp'=8,'tp'=4] {'tp'}, dimensions={2}, use_global_device_ids=true | all-gather | bytes 819200 | tf_op jit(solution)/shard_map/all_gather | solution.py:67
  58.7 3.1 %multiply_reduce_fusion = (f32[80]{0:T(128)S(1)}, f32[80,512]{1,0:T(8,128)S(1)}) fusion(bf16[4096,512]{1,0:T(8,128)(2,1)} %param.13, bf16[1,80,4096]{2,1,0:T(8,128)(2,1)S(1)} %all_gather.27), kind=kOutput, calls=%fused_computation.46 | convolution fusion | flops 335626176 | bytes 5013824 | tf_op jit(solution)/shard_map/dot_general | solution.py:70
  61.9 0.0 copy-done.1
  61.9 0.0 copy-done.5
  61.9 0.4 convolution_convert_fusion.1
  62.3 0.0 copy-done.6
  62.3 0.0 copy-start.3
  62.3 0.2 fusion.32
  62.5 1.4 %convolution_bitcast_fusion = f32[1,80,64]{1,2,0:T(8,128)S(1)} fusion(bf16[4096,64]{0,1:T(8,128)(2,1)} %param.14, bf16[1,80,4096]{2,1,0:T(8,128)(2,1)S(1)} %all_gather.27), kind=kOutput, calls=%fused_computation.21 | convolution fusion | flops 41943040 | bytes 1200128 | tf_op jit(solution)/shard_map/dot_general | solution.py:71
  63.9 0.0 copy-done.2
  63.9 0.4 convolution_convert_fusion
  64.3 0.0 copy-start.4
  64.3 0.1 fusion.40
  64.4 0.6 pad_maximum_fusion
  65.0 0.2 fusion.63
  65.3 0.1 fusion.59
  65.3 0.2 fusion.54
  65.5 0.1 fusion.61
  65.6 0.1 fusion.47
  65.7 0.3 fusion.15
  66.0 0.2 fusion.29
  66.1 0.1 fusion.55
  66.2 0.6 copy.64
  66.8 0.0 copy-done.3
  66.8 0.0 copy-done.4
  (17 shorter events, 0.1 us)
Async XLA Ops:
  0.6 27.8 %copy-start = (bf16[1,8192,64]{1,2,0:T(8,128)(2,1)S(1)}, bf16[1,8192,64]{1,2,0:T(8,128)(2,1)}, u32[]{:S(2)}) copy-start(bf16[1,8192,64]{1,2,0:T(8,128)(2,1)} %param.19) | copy-start | bytes 3145732
  2.4 47.3 %all-to-all-start = ((bf16[8,10,1024]{2,1,0:T(8,128)(2,1)}), bf16[8,10,1024]{2,1,0:T(8,128)(2,1)}, u32[]{:S(2)}, u32[]{:S(2)}) async-start(bf16[8,10,1024]{2,1,0:T(8,128)(2,1)} %copy.21), calls=%async_computation | async-start | bytes 524288 | tf_op jit(solution)/shard_map/all_to_all | solution.py:61
  22.5 6.7 %copy-start.7 = (u32[32]{0:T(128)S(1)}, u32[32]{0:T(128)}, u32[]{:S(2)}) copy-start(u32[32]{0:T(128)} %constant.87) | copy-start | bytes 388
  38.2 23.7 %copy-start.1 = (bf16[512,1024]{1,0:T(8,128)(2,1)S(1)}, bf16[512,1024]{1,0:T(8,128)(2,1)}, u32[]{:S(2)}) copy-start(bf16[512,1024]{1,0:T(8,128)(2,1)} %param.16) | copy-start | bytes 3145732
  38.2 23.7 %copy-start.5 = (f32[512]{0:T(512)S(1)}, f32[512]{0:T(512)}, u32[]{:S(2)}) copy-start(f32[512]{0:T(512)} %param.15) | copy-start | bytes 6148
  43.2 19.0 %copy-start.6 = (bf16[1,1024]{1,0:T(2,128)(2,1)S(1)}, bf16[1,1024]{1,0:T(2,128)(2,1)}, u32[]{:S(2)}) copy-start(bf16[1,1024]{1,0:T(2,128)(2,1)} %param.20) | copy-start | bytes 6148
  43.2 20.7 %copy-start.2 = (bf16[512,1024]{1,0:T(8,128)(2,1)S(1)}, bf16[512,1024]{1,0:T(8,128)(2,1)}, u32[]{:S(2)}) copy-start(bf16[512,1024]{1,0:T(8,128)(2,1)} %param.17) | copy-start | bytes 3145732
  62.3 4.5 %copy-start.3 = (bf16[80,1024]{1,0:T(8,128)(2,1)}, bf16[80,1024]{1,0:T(8,128)(2,1)S(1)}, u32[]{:S(2)}) copy-start(bf16[80,1024]{1,0:T(8,128)(2,1)S(1)} %convolution_convert_fusion.1) | copy-start | bytes 491524
  64.3 2.6 %copy-start.4 = (bf16[80,1024]{1,0:T(8,128)(2,1)}, bf16[80,1024]{1,0:T(8,128)(2,1)S(1)}, u32[]{:S(2)}) copy-start(bf16[80,1024]{1,0:T(8,128)(2,1)S(1)} %convolution_convert_fusion) | copy-start | bytes 491524
where the time goes:
time: 67.3 us; the launch traced here: 66.8 us
  blocking collectives  31.4 us (47%)
  matrix products  19.1 us (28%)
  starting transfers between devices  7.28 us (11%)
  local copies, waits for them, and re-layouts  4.87 us (7%)
  other arithmetic  2.69 us (4%)
  between operations  1.45 us (2%)
    all_gather x1, blocking collectives, on_device(): fragment = lax.all_gather(rows_here, 'tp', axis=2, tiled=True)  7.99 us
    all_to_all x1, starting transfers between devices, on_device(): lax.all_to_all(tokens, 'sp', split_axis=0, concat_axis=1, tiled=True)  7.28 us
    unnamed x1, blocking collectives  7.09 us
    dot_general x1, matrix products, on_device(): jnp.einsum('shk,spk->shp', every_latent, cached_latent_rows, preferred_el...  5.92 us
    all_gather x1, blocking collectives, combined_all(): gathered = jax.tree.map(lambda a: lax.all_gather(a, axis), part)  5.91 us
    all_gather x1, blocking collectives, on_device(): lax.all_gather(query_latent, 'tp', axis=1, tiled=True)  5.19 us
    all_gather x1, blocking collectives, on_device(): lax.all_gather(turn_own, 'tp', axis=1, tiled=True)  5.18 us
    dot_general x1, matrix products, on_device(): jnp.einsum('shp,spk->shk', local_weight.astype(jnp.bfloat16), cached_late...  5.06 us
  transfers between devices with their start and end apart: 1, of which 0 were waited for; matrix products, arithmetic and copies ran while one was open for 24% of the time, Pallas kernels for 0%

commit v1 on v0

--- a/solution.py
+++ b/solution.py
@@ -9,6 +9,17 @@
 PAST_POSITIONS = 32768
 epsilon = 1e-06
 rope_theta = 10000.0
+
+
+def split_up(x, dim, size):
+    before, after = (x.shape[:dim], x.shape[dim + 1 :])
+    return jnp.moveaxis(x.reshape(*before, size, -1, *after), dim, 0)
+
+
+def laid_out(blocks, dim):
+    lengths = list(blocks.shape[1:])
+    lengths[dim] *= blocks.shape[0]
+    return jnp.moveaxis(blocks, 0, dim).reshape(lengths)
 
 
 def combined_all(part, axis, combine):
@@ -58,7 +69,14 @@
     query_nope,
     query_rope,
 ):
-    rows_here = lax.all_to_all(tokens, "sp", split_axis=0, concat_axis=1, tiled=True)
+    count, here = (lax.axis_size("sp"), lax.axis_index("sp"))
+    blocks = split_up(tokens, 0, count)
+    outs = [blocks[here]]
+    for step in range(1, count):
+        sent = blocks[here ^ step]
+        outs.append(lax.ppermute(sent, "sp", [(i, i ^ step) for i in range(count)]))
+    blocks = jnp.stack(outs)[here ^ jnp.arange(count)]
+    rows_here = laid_out(blocks, 1)
     prompts, per_seq, features = rows_here.shape
     row_count = prompts * per_seq
     latent_width = latent_down_weight.shape[1]

time: 67.3 us -> 95.6 us (1.42)
  local copies, waits for them, and re-layouts: 4.87 us -> 23.6 us
  other arithmetic: 2.69 us -> 10.1 us
  starting transfers between devices: 7.28 us -> 12.7 us
  matrix products: 19.1 us -> 15.9 us
    ppermute x0 -> x7, starting transfers between devices: none -> 12.7 us  [on_device(): outs.append(lax.ppermute(sent, 'sp', [(i, i ^ step) for i in range(count)]))]
    unnamed x23 -> x52, local copies, waits for them, and re-layouts: 3.5 us -> 13.5 us
    all_to_all x1 -> x0, starting transfers between devices: 7.28 us -> none  [on_device(): lax.all_to_all(tokens, 'sp', split_axis=0, concat_axis=1, tiled=True)]
    exp x3, other arithmetic: 0.07 us -> 3.78 us  [combine_parts(): scale_second = jnp.exp(second[0] - highest)]
    dot_general x1, matrix products: 5.06 us -> 1.62 us  [on_device(): jnp.einsum('shp,spk->shk', local_weight.astype(jnp.bfloat16), cached_late...]
    another operation x1 -> x3, local copies, waits for them, and re-layouts: 0.08 us -> 2.66 us
    squeeze x0 -> x1, local copies, waits for them, and re-layouts: none -> 2.24 us  [on_device(): sent = blocks[here ^ step]]
    mul x3, other arithmetic: 0.03 us -> 2 us  [combine_parts(): first[2] * scale_first[..., None] + second[2] * scale_second[..., None]]
  transfers between devices with their start and end apart: 1 -> 7, of which waited for: 0 -> 1; matrix products, arithmetic and copies ran while one was open for 24% -> 37% of each run, Pallas kernels for 0% -> 0%
where the time goes in v1:
time: 95.6 us; the launch traced here: 94.9 us
  blocking collectives  30.6 us (32%)
  local copies, waits for them, and re-layouts  23.6 us (25%)
  matrix products  15.9 us (17%)
  starting transfers between devices  12.7 us (13%)
  other arithmetic  10.1 us (11%)
  between operations  1.66 us (2%)
    unnamed x52, local copies, waits for them, and re-layouts  13.5 us
    ppermute x7, starting transfers between devices, on_device(): outs.append(lax.ppermute(sent, 'sp', [(i, i ^ step) for i in range(count)]))  12.7 us
    all_gather x1, blocking collectives, on_device(): fragment = lax.all_gather(rows_here, 'tp', axis=2, tiled=True)  7.41 us
    unnamed x1, blocking collectives  7.09 us
    dot_general x1, matrix products, on_device(): jnp.einsum('shk,spk->shp', every_latent, cached_latent_rows, preferred_el...  6.05 us
    all_gather x1, blocking collectives, combined_all(): gathered = jax.tree.map(lambda a: lax.all_gather(a, axis), part)  5.76 us
    all_gather x1, blocking collectives, on_device(): lax.all_gather(query_latent, 'tp', axis=1, tiled=True)  5.19 us
    all_gather x1, blocking collectives, on_device(): lax.all_gather(turn_own, 'tp', axis=1, tiled=True)  5.18 us
  transfers between devices with their start and end apart: 7, of which 1 were waited for; matrix products, arithmetic and copies ran while one was open for 37% of the time, Pallas kernels for 0%

profile of v1, /device:TPU:0, one launch (start us, length us, event | category | flops | bytes accessed | tf_op | source)
XLA Modules:
  0.0 94.9 jit_solution(10290553117644959446)
XLA Ops:
  0.7 2.2 %constant_dynamic-slice_fusion.4 = (bf16[1,10,1024]{2,0,1:T(2,128)(2,1)S(1)}, bf16[1,10,1024]{2,0,1:T(2,128)(2,1)S(1)}, bf16[1,10,1024]{2,0,1:T(2,128)(2,1)S(1)}...) fusion(bf16[8,10,1024]{2,0,1:T(8,128)(2,1)} %param.12, ...), kind=kLoop, calls=%fused_computation.89 | loop fusion | bytes 327712 | tf_op jit(solution)/shard_map/squeeze | solution.py:76
  2.9 0.6 copy.46
  3.6 3.0 %collective-permute-start = (bf16[1,10,1024]{2,1,0:T(8,128)(2,1)}, bf16[1,10,1024]{2,1,0:T(8,128)(2,1)}, u32[]{:S(2)}, u32[]{:S(2)}) collective-permute-start(bf16[1,10,1024]{2,1,0:T(8,128)(2,1)} %copy.46), channel_id=1, source_target_pairs={{0,4},{4,0},{8,12},{12,8},{16,20},{20,16},{24,28},{28,24},{1,5},{5... | collective-permute-start | bytes 61448 | tf_op jit(solution)/shard_map/ppermute | solution.py:77
  6.5 0.6 copy.47
  7.1 1.6 %collective-permute-start.1 = (bf16[1,10,1024]{2,1,0:T(8,128)(2,1)}, bf16[1,10,1024]{2,1,0:T(8,128)(2,1)}, u32[]{:S(2)}, u32[]{:S(2)}) collective-permute-start(bf16[1,10,1024]{2,1,0:T(8,128)(2,1)} %copy.47), channel_id=1, source_target_pairs={{0,8},{4,12},{8,0},{12,4},{16,24},{20,28},{24,16},{28,20},{1,9},{5... | collective-permute-start | bytes 61448 | tf_op jit(solution)/shard_map/ppermute | solution.py:77
  8.7 0.6 copy.48
  9.3 0.6 copy.49
  10.0 3.0 %collective-permute-start.3 = (bf16[1,10,1024]{2,1,0:T(8,128)(2,1)}, bf16[1,10,1024]{2,1,0:T(8,128)(2,1)}, u32[]{:S(2)}, u32[]{:S(2)}) collective-permute-start(bf16[1,10,1024]{2,1,0:T(8,128)(2,1)} %copy.49), channel_id=1, source_target_pairs={{0,16},{4,20},{8,24},{12,28},{16,0},{20,4},{24,8},{28,12},{1,17},{... | collective-permute-start | bytes 61448 | tf_op jit(solution)/shard_map/ppermute | solution.py:77
  13.0 0.6 copy.50
  13.6 1.3 %collective-permute-start.4 = (bf16[1,10,1024]{2,1,0:T(8,128)(2,1)}, bf16[1,10,1024]{2,1,0:T(8,128)(2,1)}, u32[]{:S(2)}, u32[]{:S(2)}) collective-permute-start(bf16[1,10,1024]{2,1,0:T(8,128)(2,1)} %copy.50), channel_id=1, source_target_pairs={{0,20},{4,16},{8,28},{12,24},{16,4},{20,0},{24,12},{28,8},{1,21},{... | collective-permute-start | bytes 61448 | tf_op jit(solution)/shard_map/ppermute | solution.py:77
  14.9 0.6 add_convert_fusion
  15.4 0.7 reduce.8
  16.2 0.6 copy-done.7
  16.8 5.2 %all_gather.29 = bf16[1,32,64]{2,1,0:T(8,128)(2,1)S(1)} all-gather(bf16[1,8,64]{2,1,0:T(8,128)(2,1)S(1)} %reshape.355), channel_id=1, replica_groups=mesh['sp'=8,'tp'=4] {'tp'}, dimensions={1}, use_global_device_ids=true | all-gather | bytes 5120 | tf_op jit(solution)/shard_map/all_gather | solution.py:117
  22.0 1.8 %fusion.18 = bf16[8,1,512]{2,1,0:T(2,128)(2,1)S(1)} fusion(bf16[1,1024]{1,0:T(2,128)(2,1)} %param.20, bf16[512,1024]{1,0:T(8,128)(2,1)} %param.16), kind=kOutput, calls=%fused_computation.29 | convolution fusion | flops 1048576 | bytes 1058816 | tf_op jit(solution)/shard_map/shd,khd->shk/dot_general | solution.py:112
  23.7 5.2 %all-gather = bf16[32,512]{1,0:T(8,128)(2,1)S(1)} all-gather(bf16[8,512]{1,0:T(8,128)(2,1)S(1)} %bitcast.185), channel_id=2, replica_groups=mesh['sp'=8,'tp'=4] {'tp'}, dimensions={0}, use_global_device_ids=true | all-gather | bytes 40960 | tf_op jit(solution)/shard_map/all_gather | solution.py:116
  28.9 6.1 %fusion.11 = f32[32,8192]{1,0:T(8,128)S(1)} fusion(bf16[32,512]{1,0:T(8,128)(2,1)S(1)} %all-gather, bf16[1,8192,512]{2,1,0:T(8,128)(2,1)} %param.18), kind=kOutput, calls=%fused_computation.18 | convolution fusion | flops 268435456 | bytes 9469952 | tf_op jit(solution)/shard_map/shk,spk->shp/dot_general | solution.py:119
  35.0 0.4 fusion.66
  35.4 0.4 fusion.23
  35.8 1.6 %fusion.9 = f32[32,512]{1,0:T(8,128)S(1)} fusion(bf16[1,8192,512]{2,1,0:T(8,128)(2,1)S(1)} %bitcast.180, f32[32,8192]{1,0:T(8,128)S(1)} %get-tuple-element.238, f32[32]{0:T(128)S(1)} %get-tuple-element.237), kind=kOutput, calls=%fused_computation.16 | convolution fusion | flops 268959744 | bytes 9502848 | tf_op jit(solution)/shard_map/shp,spk->shk/dot_general | solution.py:129
  37.5 0.6 dynamic-slice.11
  38.7 0.2 dynamic-update-slice
  39.0 0.2 dynamic-update-slice.1
  39.2 7.1 %all-reduce.2 = (f32[128]{0:T(128)S(1)}, f32[128]{0:T(128)S(1)}) all-reduce(f32[128]{0:T(128)S(1)} %dynamic-update-slice, f32[128]{0:T(128)S(1)} %dynamic-update-slice.1), channel_id=3, replica_groups=mesh['sp'=8,'tp'=4] {'tp'}, use_global_device_ids=true, to_apply=%add | all-reduce | flops 256 | bytes 2048
  46.3 0.7 reshape.375
  46.9 0.6 slice_bitcast_fusion.1
  47.5 0.7 reshape.376
  48.2 0.6 pad_clamp_fusion
  48.8 0.6 fusion.35
  49.4 5.8 %all-gather.3 = f32[128,512]{1,0:T(8,128)S(1)} all-gather(f32[32,512]{1,0:T(8,128)S(1)} %fusion.9), channel_id=5, replica_groups=mesh['sp'=8,'tp'=4] {'tp'}, dimensions={0}, use_global_device_ids=true | all-gather | bytes 327680 | tf_op jit(solution)/shard_map/all_gather | solution.py:26
  55.2 7.6 %while.19 = (s32[]{:T(128)}, f32[1,32]{1,0:T(1,128)}, f32[1,32]{1,0:T(1,128)}, f32[1,32,512]{2,1,0:T(8,128)S(1)}, f32[4,1,32]{2,1,0:T(1,128)}, /*index=5*/f32[4,...) while((s32[]{:T(128)}, f32[1,32]{1,0:T(1,128)}, f32[1,32]{1,0:T(1,128)}, ...), condition=%wide.region_4.5_spmd, body=%wide.region_3.4_spmd.sunk | while | flops 49381 | bytes 198675 | solution.py:31
  55.2 0.7 fusion.80
  55.8 1.3 %fusion.81 = (f32[32]{0:T(128)S(1)}, f32[1,32]{1,0:T(1,128)}) fusion(f32[1,32]{1,0:T(1,128)S(1)} %get-tuple-element.313, f32[4,1,32]{2,1,0:T(1,128)} %get-tuple-element.316, s32[]{:T(128)S(6)} %select_n.70, f32[4,1,32]{2,1,0:T(1,128)} %get-tuple-element.317, f32[1,32]{1,0:T(1,128)} %get-tuple-element.304, f32[1,32]{1,0:T(1,128)} %get-tuple-element.303), kind=kLoop, calls=%fused_computation.13.clone.1 | loop fusion | flops 160 | bytes 900 | tf_op jit(solution)/shard_map/while/body/eval_jaxpr/exp | solution.py:54
  57.1 0.5 copy.103
  57.7 0.7 fusion.80
  58.4 1.3 %fusion.81 = (f32[32]{0:T(128)S(1)}, f32[1,32]{1,0:T(1,128)}) fusion(f32[1,32]{1,0:T(1,128)S(1)} %get-tuple-element.313, f32[4,1,32]{2,1,0:T(1,128)} %get-tuple-element.316, s32[]{:T(128)S(6)} %select_n.70, f32[4,1,32]{2,1,0:T(1,128)} %get-tuple-element.317, f32[1,32]{1,0:T(1,128)} %get-tuple-element.304, f32[1,32]{1,0:T(1,128)} %get-tuple-element.303), kind=kLoop, calls=%fused_computation.13.clone.1 | loop fusion | flops 160 | bytes 900 | tf_op jit(solution)/shard_map/while/body/eval_jaxpr/exp | solution.py:54
  59.6 0.5 copy.103
  60.2 0.7 fusion.80
  60.9 1.3 %fusion.81 = (f32[32]{0:T(128)S(1)}, f32[1,32]{1,0:T(1,128)}) fusion(f32[1,32]{1,0:T(1,128)S(1)} %get-tuple-element.313, f32[4,1,32]{2,1,0:T(1,128)} %get-tuple-element.316, s32[]{:T(128)S(6)} %select_n.70, f32[4,1,32]{2,1,0:T(1,128)} %get-tuple-element.317, f32[1,32]{1,0:T(1,128)} %get-tuple-element.304, f32[1,32]{1,0:T(1,128)} %get-tuple-element.303), kind=kLoop, calls=%fused_computation.13.clone.1 | loop fusion | flops 160 | bytes 900 | tf_op jit(solution)/shard_map/while/body/eval_jaxpr/exp | solution.py:54
  62.2 0.5 copy.103
  62.8 0.5 multiply_power_fusion
  63.3 1.3 %reshape.359 = bf16[8,64]{1,0:T(8,128)(2,1)} reshape(bf16[512]{0:T(512)(128)(2,1)} %copy-done.7) | data formatting | bytes 2048 | tf_op jit(solution)/shard_map/reshape.46
  64.7 3.7 %collective-permute-start.5 = (bf16[1,10,1024]{2,1,0:T(8,128)(2,1)S(1)}, bf16[1,10,1024]{2,1,0:T(8,128)(2,1)S(1)}, u32[]{:S(2)}, u32[]{:S(2)}) collective-permute-start(bf16[1,10,1024]{2,1,0:T(8,128)(2,1)S(1)} %copy.51), channel_id=1, source_target_pairs={{0,24},{4,28},{8,16},{12,20},{16,8},{20,12},{24,0},{28,4},{1,25},{... | collective-permute-start | bytes 61448 | tf_op jit(solution)/shard_map/ppermute | solution.py:77
  68.4 1.4 %bitcast_dynamic-update-slice_fusion.6 = bf16[8,1,10,1024]{3,2,1,0:T(8,128)(2,1)} fusion(bf16[8,1,10,1024]{3,2,1,0:T(8,128)(2,1)} %fusion.35, bf16[1,10,1024]{2,1,0:T(8,128)(2,1)} %collective-permute-done), kind=kLoop, calls=%fused_computation.57 | loop fusion | bytes 65536
  69.8 0.2 collective-permute-start.6
  70.0 1.4 %bitcast_dynamic-update-slice_fusion.5 = bf16[8,1,10,1024]{3,2,1,0:T(8,128)(2,1)} fusion(bf16[8,1,10,1024]{3,2,1,0:T(8,128)(2,1)} %bitcast_dynamic-update-slice_fusion.6, bf16[1,10,1024]{2,1,0:T(8,128)(2,1)} %collective-permute-done.1), kind=kLoop, calls=%fused_computation.56 | loop fusion | bytes 65536
  71.3 1.4 %bitcast_dynamic-update-slice_fusion.4 = bf16[8,1,10,1024]{3,2,1,0:T(8,128)(2,1)} fusion(bf16[8,1,10,1024]{3,2,1,0:T(8,128)(2,1)} %bitcast_dynamic-update-slice_fusion.5, bf16[1,10,1024]{2,1,0:T(8,128)(2,1)} %collective-permute-done.2), kind=kLoop, calls=%fused_computation.55 | loop fusion | bytes 65536
  72.7 1.4 %bitcast_dynamic-update-slice_fusion.3 = bf16[8,1,10,1024]{3,2,1,0:T(8,128)(2,1)} fusion(bf16[8,1,10,1024]{3,2,1,0:T(8,128)(2,1)} %bitcast_dynamic-update-slice_fusion.4, bf16[1,10,1024]{2,1,0:T(8,128)(2,1)} %collective-permute-done.3), kind=kLoop, calls=%fused_computation.54 | loop fusion | bytes 65536
  74.1 1.4 %bitcast_dynamic-update-slice_fusion.2 = bf16[8,1,10,1024]{3,2,1,0:T(8,128)(2,1)} fusion(bf16[8,1,10,1024]{3,2,1,0:T(8,128)(2,1)} %bitcast_dynamic-update-slice_fusion.3, bf16[1,10,1024]{2,1,0:T(8,128)(2,1)} %collective-permute-done.4), kind=kLoop, calls=%fused_computation.53 | loop fusion | bytes 65536
  75.5 0.6 bitcast_dynamic-update-slice_fusion.1
  76.1 0.3 collective-permute-done.6
  76.4 0.6 bitcast_dynamic-update-slice_fusion
  77.0 1.6 %gather_fusion = bf16[8,10,1024]{2,1,0:T(8,128)(2,1)S(1)} fusion(bf16[8,10,1024]{2,1,0:T(8,128)(2,1)} %bitcast.182, s32[1024]{0:T(1024)} %pad_clamp_fusion), kind=kCustom, calls=%fused_computation | custom fusion | bytes 327712 | tf_op jit(solution)/shard_map/gather | solution.py:78
  78.6 0.7 reshape_transpose.3
  79.4 7.4 %all_gather.27 = bf16[1,80,4096]{2,1,0:T(8,128)(2,1)S(1)} all-gather(bf16[1,80,1024]{2,1,0:T(8,128)(2,1)} %reshape_transpose.3), channel_id=1, replica_groups=mesh['sp'=8,'tp'=4] {'tp'}, dimensions={2}, use_global_device_ids=true | all-gather | bytes 819200 | tf_op jit(solution)/shard_map/all_gather | solution.py:85
  86.8 1.4 %convolution_bitcast_fusion = f32[1,80,64]{1,2,0:T(8,128)S(1)} fusion(bf16[4096,64]{0,1:T(8,128)(2,1)} %param.14, bf16[1,80,4096]{2,1,0:T(8,128)(2,1)S(1)} %all_gather.27), kind=kOutput, calls=%fused_computation.22 | convolution fusion | flops 41943040 | bytes 1200128 | tf_op jit(solution)/shard_map/dot_general | solution.py:89
  88.2 3.1 %multiply_reduce_fusion = (f32[80]{0:T(128)S(1)}, f32[80,512]{1,0:T(8,128)S(1)}) fusion(bf16[4096,512]{1,0:T(8,128)(2,1)} %param.13, bf16[1,80,4096]{2,1,0:T(8,128)(2,1)S(1)} %all_gather.27), kind=kOutput, calls=%fused_computation.47 | convolution fusion | flops 335626176 | bytes 5013824 | tf_op jit(solution)/shard_map/dot_general | solution.py:88
  91.3 0.4 convolution_convert_fusion.1
  91.7 0.4 convolution_convert_fusion
  92.5 0.6 pad_maximum_fusion
  93.1 0.2 fusion.65
  93.4 0.2 fusion.55
  93.7 0.3 fusion.15
  94.2 0.6 copy.84
  (58 shorter events, 1.3 us)
Async XLA Ops:
  0.6 34.4 %copy-start = (bf16[1,8192,64]{1,2,0:T(8,128)(2,1)S(1)}, bf16[1,8192,64]{1,2,0:T(8,128)(2,1)}, u32[]{:S(2)}) copy-start(bf16[1,8192,64]{1,2,0:T(8,128)(2,1)} %param.19) | copy-start | bytes 3145732
  3.6 61.2 %collective-permute-start = (bf16[1,10,1024]{2,1,0:T(8,128)(2,1)}, bf16[1,10,1024]{2,1,0:T(8,128)(2,1)}, u32[]{:S(2)}, u32[]{:S(2)}) collective-permute-start(bf16[1,10,1024]{2,1,0:T(8,128)(2,1)} %copy.46), channel_id=1, source_target_pairs={{0,4},{4,0},{8,12},{12,8},{16,20},{20,16},{24,28},{28,24},{1,5},{5... | collective-permute-start | bytes 61448 | tf_op jit(solution)/shard_map/ppermute | solution.py:77
  7.1 62.6 %collective-permute-start.1 = (bf16[1,10,1024]{2,1,0:T(8,128)(2,1)}, bf16[1,10,1024]{2,1,0:T(8,128)(2,1)}, u32[]{:S(2)}, u32[]{:S(2)}) collective-permute-start(bf16[1,10,1024]{2,1,0:T(8,128)(2,1)} %copy.47), channel_id=1, source_target_pairs={{0,8},{4,12},{8,0},{12,4},{16,24},{20,28},{24,16},{28,20},{1,9},{5... | collective-permute-start | bytes 61448 | tf_op jit(solution)/shard_map/ppermute | solution.py:77
  9.3 62.0 %collective-permute-start.2 = (bf16[1,10,1024]{2,1,0:T(8,128)(2,1)}, bf16[1,10,1024]{2,1,0:T(8,128)(2,1)}, u32[]{:S(2)}, u32[]{:S(2)}) collective-permute-start(bf16[1,10,1024]{2,1,0:T(8,128)(2,1)} %copy.48), channel_id=1, source_target_pairs={{0,12},{4,8},{8,4},{12,0},{16,28},{20,24},{24,20},{28,16},{1,13},{... | collective-permute-start | bytes 61448 | tf_op jit(solution)/shard_map/ppermute | solution.py:77
  10.0 62.7 %collective-permute-start.3 = (bf16[1,10,1024]{2,1,0:T(8,128)(2,1)}, bf16[1,10,1024]{2,1,0:T(8,128)(2,1)}, u32[]{:S(2)}, u32[]{:S(2)}) collective-permute-start(bf16[1,10,1024]{2,1,0:T(8,128)(2,1)} %copy.49), channel_id=1, source_target_pairs={{0,16},{4,20},{8,24},{12,28},{16,0},{20,4},{24,8},{28,12},{1,17},{... | collective-permute-start | bytes 61448 | tf_op jit(solution)/shard_map/ppermute | solution.py:77
  13.6 60.5 %collective-permute-start.4 = (bf16[1,10,1024]{2,1,0:T(8,128)(2,1)}, bf16[1,10,1024]{2,1,0:T(8,128)(2,1)}, u32[]{:S(2)}, u32[]{:S(2)}) collective-permute-start(bf16[1,10,1024]{2,1,0:T(8,128)(2,1)} %copy.50), channel_id=1, source_target_pairs={{0,20},{4,16},{8,28},{12,24},{16,4},{20,0},{24,12},{28,8},{1,21},{... | collective-permute-start | bytes 61448 | tf_op jit(solution)/shard_map/ppermute | solution.py:77
  16.1 0.6 copy-start.7
  22.0 13.8 %slice-start = ((s8[8388608]{0:T(1024)(128)(4,1)}), s8[4194304]{0:T(1024)(128)(4,1)S(1)}, s32[]{:S(2)}) async-start(s8[8388608]{0:T(1024)(128)(4,1)} %bitcast.179), calls=%async_computation | async-start | bytes 8388608
  28.9 6.8 %slice-start.1 = ((s8[8388608]{0:T(1024)(128)(4,1)}), s8[4194304]{0:T(1024)(128)(4,1)S(1)}, s32[]{:S(2)}) async-start(s8[8388608]{0:T(1024)(128)(4,1)} %bitcast.179), calls=%async_computation.1 | async-start | bytes 8388608
  35.8 1.7 %copy-start.13 = (u32[32]{0:T(128)S(1)}, u32[32]{0:T(128)}, u32[]{:S(2)}) copy-start(u32[32]{0:T(128)} %constant.107) | copy-start | bytes 388
  37.4 53.9 %copy-start.1 = (bf16[512,1024]{1,0:T(8,128)(2,1)S(1)}, bf16[512,1024]{1,0:T(8,128)(2,1)}, u32[]{:S(2)}) copy-start(bf16[512,1024]{1,0:T(8,128)(2,1)} %param.16) | copy-start | bytes 3145732
  37.4 54.3 %copy-start.2 = (bf16[512,1024]{1,0:T(8,128)(2,1)S(1)}, bf16[512,1024]{1,0:T(8,128)(2,1)}, u32[]{:S(2)}) copy-start(bf16[512,1024]{1,0:T(8,128)(2,1)} %param.17) | copy-start | bytes 3145732
  64.6 26.7 %copy-start.8 = (f32[512]{0:T(512)S(1)}, f32[512]{0:T(512)}, u32[]{:S(2)}) copy-start(f32[512]{0:T(512)} %param.15) | copy-start | bytes 6148
  64.6 27.4 %copy-start.12 = (bf16[1,1024]{1,0:T(2,128)(2,1)S(1)}, bf16[1,1024]{1,0:T(2,128)(2,1)}, u32[]{:S(2)}) copy-start(bf16[1,1024]{1,0:T(2,128)(2,1)} %param.20) | copy-start | bytes 6148
  64.6 27.6 %copy-start.10 = (f32[80]{0:T(128)S(1)}, f32[80]{0:T(128)}, u32[]{:S(2)}) copy-start(f32[80]{0:T(128)} %add_convert_fusion) | copy-start | bytes 964
  64.7 27.6 %copy-start.11 = (f32[32]{0:T(128)S(1)}, f32[32]{0:T(128)}, u32[]{:S(2)}) copy-start(f32[32]{0:T(128)} %multiply_power_fusion) | copy-start | bytes 388
  64.7 28.4 %copy-start.9 = (bf16[8,64]{1,0:T(8,128)(2,1)S(1)}, bf16[8,64]{1,0:T(8,128)(2,1)}, u32[]{:S(2)}) copy-start(bf16[8,64]{1,0:T(8,128)(2,1)} %reshape.359) | copy-start | bytes 3076
  64.7 28.6 %copy-start.5 = (f32[1,32]{1,0:T(1,128)S(1)}, f32[1,32]{1,0:T(1,128)}, u32[]{:S(2)}) copy-start(f32[1,32]{1,0:T(1,128)} %get-tuple-element.183) | copy-start | bytes 388
  64.7 28.9 %copy-start.6 = (f32[1,32]{1,0:T(1,128)S(1)}, f32[1,32]{1,0:T(1,128)}, u32[]{:S(2)}) copy-start(f32[1,32]{1,0:T(1,128)} %get-tuple-element.184) | copy-start | bytes 388
  64.7 10.7 %collective-permute-start.5 = (bf16[1,10,1024]{2,1,0:T(8,128)(2,1)S(1)}, bf16[1,10,1024]{2,1,0:T(8,128)(2,1)S(1)}, u32[]{:S(2)}, u32[]{:S(2)}) collective-permute-start(bf16[1,10,1024]{2,1,0:T(8,128)(2,1)S(1)} %copy.51), channel_id=1, source_target_pairs={{0,24},{4,28},{8,16},{12,20},{16,8},{20,12},{24,0},{28,4},{1,25},{... | collective-permute-start | bytes 61448 | tf_op jit(solution)/shard_map/ppermute | solution.py:77
  69.8 6.6 %collective-permute-start.6 = (bf16[1,10,1024]{2,1,0:T(8,128)(2,1)S(1)}, bf16[1,10,1024]{2,1,0:T(8,128)(2,1)S(1)}, u32[]{:S(2)}, u32[]{:S(2)}) collective-permute-start(bf16[1,10,1024]{2,1,0:T(8,128)(2,1)S(1)} %copy.52), channel_id=1, source_target_pairs={{0,28},{4,24},{8,20},{12,16},{16,12},{20,8},{24,4},{28,0},{1,29},{... | collective-permute-start | bytes 61448 | tf_op jit(solution)/shard_map/ppermute | solution.py:77
  91.7 3.2 %copy-start.3 = (bf16[80,1024]{1,0:T(8,128)(2,1)}, bf16[80,1024]{1,0:T(8,128)(2,1)S(1)}, u32[]{:S(2)}) copy-start(bf16[80,1024]{1,0:T(8,128)(2,1)S(1)} %convolution_convert_fusion.1) | copy-start | bytes 491524
  92.1 2.8 %copy-start.4 = (bf16[80,1024]{1,0:T(8,128)(2,1)}, bf16[80,1024]{1,0:T(8,128)(2,1)S(1)}, u32[]{:S(2)}) copy-start(bf16[80,1024]{1,0:T(8,128)(2,1)S(1)} %convolution_convert_fusion) | copy-start | bytes 491524
